TPU v7x, 32 devices: a whole 2x2x4 slice. The times are simulated.
32 devices in a mesh: sp: 8 (over z, x), tp: 4 (over y, core).
Axes of the slice: x: 2, y: 2, z: 4, core: 2. Of those that a mesh axis runs over, the one named last changes fastest.
Arguments:
- residual: bfloat16 [1536, 2048], P('sp', 'tp'), may hold values from -10 to 10
- queries: bfloat16 [1536, 16, 128], P('sp', 'tp'), may hold values from -6.5 to 6.5
- key_rows: bfloat16 [1536, 16, 128], P('sp', 'tp'), may hold values from -6.5 to 6.5
- value_rows: bfloat16 [1536, 16, 128], P('sp', 'tp'), may hold values from -6 to 6
- diff_scale: float32 [16], P('tp'), may hold values from 0.3 to 0.8
- head_gain: float32 [128], replicated, may hold values from 0.1 to 1.9
- out_weight: bfloat16 [2048, 2048], P(None, 'tp'), may hold values from -0.125 to 0.125
- norm_gain: float32 [2048], replicated, may hold values from 0.1 to 1.9
- gate_weight: bfloat16 [8, 2048, 4096], P('sp', None, 'tp'), may hold values from -0.5 to 0.5
- up_weight: bfloat16 [8, 2048, 4096], P('sp', None, 'tp'), may hold values from -0.5 to 0.5
- down_weight: bfloat16 [8, 4096, 2048], P('sp', None, 'tp'), may hold values from -0.01171875 to 0.01171875
- expert_ids: int32 [1536, 2], P('sp'), may hold values from 0 to 7, all different within a row; in each aligned block of 192 rows (0 to 191, 192 to 383, ...) at most 96 rows name the same one
- route_logit: float32 [1536, 2], P('sp'), may hold values from -6 to 6
Outputs:
- updated: bfloat16 [1536, 2048], P('sp', 'tp')
Inputs may be any that keep to these rules, and one draw needn't show every extreme that they name: `expert_ids`: A token's 2 experts differ. The 192 tokens of one index of sp name one expert at most 96 times, a bound that some block reaches on some index.
All inputs are finite; a program needn't handle non-finite values.
Results may differ from a plain program's by a relative error of at most 0.014.
Values may be sent and summed in bfloat16 or wider, within the bound.
A program may use at most 64 MiB of HBM per device.

v0:
```python
import math
import jax
import jax.numpy as jnp
from jax import lax
from jax.sharding import PartitionSpec as P

D = 2048
QK = 64
SPAN = 64
NORM_EPS = 1e-05
CLAMP_LIMIT = 7.0
SWISH_ALPHA = 1.702
HEAD_KEEP = 0.8
NEG_FILL = -1e30


def update_map(running, query_half, key_half, value_block, visible):
    row_peak, row_total, accum = running
    scores = jnp.einsum(
        "qhd,khd->hqk", query_half, key_half, preferred_element_type=jnp.float32
    ) * QK ** (-0.5)
    scores = jnp.where(visible[None], scores, NEG_FILL)
    new_peak = jnp.maximum(row_peak, jnp.max(scores, axis=-1))
    exp_weights = jnp.where(visible[None], jnp.exp(scores - new_peak[..., None]), 0.0)
    rescale = jnp.exp(row_peak - new_peak)
    row_total = row_total * rescale + jnp.sum(exp_weights, axis=-1)
    accum = accum * rescale[..., None] + jnp.einsum(
        "hqk,khv->hqv",
        exp_weights.astype(jnp.bfloat16),
        value_block,
        preferred_element_type=jnp.float32,
    )
    return (new_peak, row_total, accum)


def local(
    residual,
    queries,
    key_rows,
    value_rows,
    diff_scale,
    head_gain,
    out_weight,
    norm_gain,
    gate_weight,
    up_weight,
    down_weight,
    expert_ids,
    route_logit,
):
    tokens_here = queries.shape[0]
    heads_here = queries.shape[1]
    value_width = value_rows.shape[2]
    query_start = lax.axis_index("sp") * tokens_here
    query_span = (query_start + jnp.arange(tokens_here, dtype=jnp.int32)) // SPAN
    first_query = queries[..., :QK]
    second_query = queries[..., QK:]
    empty_map = (
        jnp.full((heads_here, tokens_here), NEG_FILL, jnp.float32),
        jnp.zeros((heads_here, tokens_here), jnp.float32),
        jnp.zeros((heads_here, tokens_here, value_width), jnp.float32),
    )
    folded = (empty_map, empty_map)
    key_piece = lax.all_gather(key_rows, "sp", axis=0, tiled=True)
    value_piece = lax.all_gather(value_rows, "sp", axis=0, tiled=True)
    key_count = key_piece.shape[0]
    key_width = math.gcd(key_count, 1024)
    blocks = key_count // key_width
    key_blocks = key_piece.reshape(blocks, key_width, heads_here, 2 * QK)
    value_blocks = value_piece.reshape(blocks, key_width, heads_here, value_width)

    def advance(running, inputs):
        block_index, key_block, value_block = inputs
        key_start = block_index * key_width

        def compute(current):
            key_span = (key_start + jnp.arange(key_width, dtype=jnp.int32)) // SPAN
            visible = key_span[None, :] <= query_span[:, None]
            first = update_map(current[0], first_query, key_block[..., :QK], value_block, visible)
            second = update_map(current[1], second_query, key_block[..., QK:], value_block, visible)
            return (first, second)

        running = lax.cond(
            key_start < query_start + tokens_here, compute, lambda current: current, running
        )
        return (running, None)

    folded, _ = lax.scan(
        advance, folded, (jnp.arange(blocks, dtype=jnp.int32), key_blocks, value_blocks)
    )
    first_map, second_map = folded
    mixture = (
        first_map[2] / first_map[1][..., None]
        - diff_scale[:, None, None] * second_map[2] / second_map[1][..., None]
    )
    scale_back = lax.rsqrt(jnp.mean(mixture * mixture, axis=-1, keepdims=True) + NORM_EPS)
    attended = (mixture * scale_back * head_gain * HEAD_KEEP).astype(jnp.bfloat16)
    column_width = out_weight.shape[1]
    head_weight = out_weight.reshape(-1, value_width, column_width)
    weight_slice = head_weight
    projected = jnp.einsum(
        "htv,hvd->td",
        lax.all_gather(attended, "tp", axis=0, tiled=True),
        weight_slice,
        preferred_element_type=jnp.float32,
    )
    after_mixer = (residual.astype(jnp.float32) + projected).astype(jnp.bfloat16)
    mixer_float = after_mixer.astype(jnp.float32)
    partial_value = jnp.sum(mixer_float * mixer_float, axis=-1)
    square_total = lax.psum(partial_value, "tp")
    gain_slice = lax.dynamic_slice_in_dim(
        norm_gain, lax.axis_index("tp") * column_width, column_width, 0
    )
    normed = (mixer_float * lax.rsqrt(square_total / D + NORM_EPS)[:, None] * gain_slice).astype(
        jnp.bfloat16
    )
    experts = lax.axis_size("sp")
    top_count = expert_ids.shape[1]
    capacity = 2 * tokens_here * top_count // experts
    chosen = expert_ids.reshape(-1)
    onehot = (chosen[:, None] == jnp.arange(experts, dtype=jnp.int32)[None, :]).astype(jnp.int32)
    rank_in = jnp.sum(jnp.cumsum(onehot, axis=0) * onehot, axis=1) - 1
    slot_index = chosen * capacity + rank_in
    owner_row = (
        jnp.full((experts * capacity,), tokens_here, jnp.int32)
        .at[slot_index]
        .set(jnp.arange(tokens_here * top_count, dtype=jnp.int32) // top_count)
    )
    padded = jnp.concatenate([normed, jnp.zeros((1, normed.shape[1]), jnp.bfloat16)], axis=0)
    outgoing = padded[owner_row].reshape(experts, capacity, normed.shape[1])
    expert_input = lax.all_gather(
        lax.all_to_all(outgoing, "sp", split_axis=0, concat_axis=0, tiled=True),
        "tp",
        axis=2,
        tiled=True,
    )
    sources = expert_input.shape[0]
    items = expert_input.shape[1]
    flat_rows = expert_input.reshape(sources * items, -1)
    pre_gate = jnp.dot(flat_rows, gate_weight[0], preferred_element_type=jnp.float32)
    pre_up = jnp.dot(flat_rows, up_weight[0], preferred_element_type=jnp.float32)
    capped = jnp.minimum(pre_gate, CLAMP_LIMIT)
    linear = jnp.clip(pre_up, -CLAMP_LIMIT, CLAMP_LIMIT)
    hidden = (capped * jax.nn.sigmoid(SWISH_ALPHA * capped) * (linear + 1.0)).astype(jnp.bfloat16)
    weight_slice = down_weight[0]
    expert_out = jnp.dot(
        lax.all_gather(hidden, "tp", axis=1, tiled=True),
        weight_slice,
        preferred_element_type=jnp.float32,
    )
    expert_out = expert_out.astype(jnp.bfloat16).reshape(sources, items, -1)
    returned_rows = lax.all_to_all(expert_out, "sp", split_axis=0, concat_axis=0, tiled=True)
    picked = returned_rows.reshape(experts * capacity, -1)[slot_index].astype(jnp.float32)
    picked = picked.reshape(tokens_here, top_count, -1)
    weights = jax.nn.softmax(route_logit, axis=-1)
    routed = jnp.sum(picked * weights[..., None], axis=1)
    return (mixer_float + routed).astype(jnp.bfloat16)


def solution(mesh):
    return jax.shard_map(
        local,
        mesh=mesh,
        in_specs=(
            P("sp", "tp"),
            P("sp", "tp", None),
            P("sp", "tp", None),
            P("sp", "tp", None),
            P("tp"),
            P(),
            P(None, "tp"),
            P(),
            P("sp", None, "tp"),
            P("sp", None, "tp"),
            P("sp", None, "tp"),
            P("sp", None),
            P("sp", None),
        ),
        out_specs=P("sp", "tp"),
        check_vma=False,
    )
```

profile of v0, /device:TPU:0, one launch (start us, length us, event | category | flops | bytes accessed | tf_op | source)
XLA Modules:
  0.0 296.3 jit_solution(3500172858010482587)
XLA Ops:
  6.5 1.8 copy.27
  8.4 1.6 copy.29
  10.1 0.8 copy.34
  10.9 0.1 eq.29
  11.1 0.1 eq.25
  11.2 0.2 fusion.56
  11.4 0.1 copy.37
  11.6 0.1 copy.38
  11.8 0.9 reduce-window.6
  12.6 0.2 slice_reduce_fusion
  13.0 0.1 mul.173
  13.2 0.8 dynamic_slice.28
  14.1 2.9 scatter_custom_fusion
  17.0 39.5 %all-gather.5.cloned.1.call-done = bf16[1536,4,128]{2,0,1:T(8,128)(2,1)} async-done(((bf16[192,4,128]{2,0,1:T(8,128)(2,1)}), bf16[1536,4,128]{2,0,1:T(8,128)(2,1)}) %all-gather.5.cloned.1.call-update) | async-done | bytes 1572880 | tf_op jit(solution)/shard_map/all_gather | solution.py:64
  56.5 2.6 copy.31
  59.1 42.2 %all-gather.7.cloned.1.call-done = bf16[1536,4,128]{2,0,1:T(8,128)(2,1)} async-done(((bf16[192,4,128]{2,0,1:T(8,128)(2,1)}), bf16[1536,4,128]{2,0,1:T(8,128)(2,1)}) %all-gather.7.cloned.1.call-update) | async-done | bytes 1572880 | tf_op jit(solution)/shard_map/all_gather | solution.py:65
  101.2 2.7 copy.32
  104.0 9.0 %while.23 = (s32[]{:T(128)}, f32[4,192]{1,0:T(4,128)S(1)}, f32[4,192]{1,0:T(4,128)S(1)}, f32[4,192,128]{2,1,0:T(8,128)S(1)}, f32[4,192]{1,0:T(4,128)S(1)}, /*ind...) while((s32[]{:T(128)}, f32[4,192]{1,0:T(4,128)S(1)}, ...), condition=%wide.region_7.8_spmd.clone, body=%wide.region_0.7_spmd.clone.sunk | while | flops 309574784 | bytes 20891532 | solution.py:88
  104.1 0.6 dynamic_slice.42
  105.4 5.0 %conditional.3 = ((f32[4,192]{1,0:T(4,128)S(1)}, f32[4,192]{1,0:T(4,128)S(1)}, f32[4,192,128]{2,1,0:T(8,128)S(1)}, f32[4,192]{1,0:T(4,128)S(1)}, f32[4,192]{1,0:T(4,128)S(1)}, /*index=5*/f32[4,192,128]{2,1,0:T(8,128)S(1)})) conditional(s32[]{:T(128)} %convert_element_type.82, (f32[4,192]{1,0:T(4,128)S(1)}, f32[4,192]{1,0:T(4,128)S(1)}, ...), branch_computations={%region_1.1_spmd, %region_2.6_spmd.clone} | conditional | flops 309572096 | bytes 20887848 | solution.py:83
  105.5 1.1 dynamic-slice_bitcast_fusion
  106.6 0.6 fusion.54
  107.2 0.6 fusion.55
  107.8 1.2 fusion.5
  109.0 0.2 copy-done.1
  109.2 0.6 convolution_add_fusion
  109.7 0.6 convolution_add_fusion.1
  110.4 0.6 dynamic_slice.42
  111.7 0.6 dynamic_slice.42
  113.1 0.5 multiply_reduce_fusion.2
  113.6 0.2 multiply_convert_fusion.2
  113.7 8.6 %all_gather.17 = bf16[16,192,128]{2,1,0:T(8,128)(2,1)S(1)} all-gather(bf16[4,192,128]{2,1,0:T(8,128)(2,1)S(1)} %multiply_convert_fusion.2), channel_id=1, replica_groups=mesh['sp'=8,'tp'=4] {'tp'}, dimensions={0}, use_global_device_ids=true | all-gather | bytes 983040 | tf_op jit(solution)/shard_map/all_gather | solution.py:103
  122.3 0.7 multiply_reduce_fusion.1
  123.0 6.2 %psum.7 = f32[192]{0:T(256)S(1)} all-reduce(f32[192]{0:T(256)S(1)} %get-tuple-element.467), channel_id=1, replica_groups=mesh['sp'=8,'tp'=4] {'tp'}, use_global_device_ids=true, to_apply=%region_10.11 | all-reduce | flops 192 | bytes 1536 | tf_op jit(solution)/shard_map/psum | solution.py:110
  129.3 2.7 gather_fusion
  132.0 32.5 %all_to_all.10 = bf16[8,96,512]{2,1,0:T(8,128)(2,1)} all-to-all(bf16[8,96,512]{2,1,0:T(8,128)(2,1)S(1)} %bitcast.62), channel_id=1, replica_groups=mesh['sp'=8,'tp'=4] {'sp'}, dimensions={0} | all-to-all | bytes 1572864 | tf_op jit(solution)/shard_map/all_to_all | solution.py:132
  164.5 0.2 all-gather.11.cloned.1.call-start
  164.7 26.5 %all-gather.9.cloned.1.call-done = bf16[8,96,2048]{2,1,0:T(8,128)(2,1)} async-done(((bf16[8,96,512]{2,1,0:T(8,128)(2,1)}), bf16[8,96,2048]{2,1,0:T(8,128)(2,1)}) %all-gather.9.cloned.1.call-update) | async-done | bytes 3145744 | tf_op jit(solution)/shard_map/all_gather | solution.py:131
  191.3 6.3 %fusion.32 = f32[768,1024]{1,0:T(8,128)S(1)} fusion(bf16[768,2048]{1,0:T(8,128)(2,1)} %bitcast.67, bf16[1,2048,1024]{2,1,0:T(8,128)(2,1)} %param.26), kind=kOutput, calls=%fused_computation.55 | convolution fusion | flops 3221225472 | bytes 10485760 | tf_op jit(solution)/shard_map/dot_general | solution.py:141
  197.6 5.3 %multiply_convert_fusion = bf16[768,1024]{1,0:T(8,128)(2,1)} fusion(f32[768,1024]{1,0:T(8,128)S(1)} %fusion.32, bf16[768,2048]{1,0:T(8,128)(2,1)S(1)} %bitcast.68, bf16[1,2048,1024]{2,1,0:T(8,128)(2,1)S(1)} %copy-done.8), kind=kOutput, calls=%fused_computation.59 | convolution fusion | flops 3229089792 | bytes 12058624 | tf_op jit(solution)/shard_map/dot_general | solution.py:140
  202.9 46.5 %all-gather.11.cloned.1.call-done = bf16[768,4096]{1,0:T(8,128)(2,1)} async-done(((bf16[768,1024]{1,0:T(8,128)(2,1)}), bf16[768,4096]{1,0:T(8,128)(2,1)}) %all-gather.11.cloned.1.call-update) | async-done | bytes 6291472 | tf_op jit(solution)/shard_map/all_gather | solution.py:147
  249.4 8.3 %fusion.38 = bf16[768,512]{1,0:T(8,128)(2,1)} fusion(bf16[768,4096]{1,0:T(8,128)(2,1)} %all-gather.11.cloned.1.call-done, bf16[1,4096,512]{2,1,0:T(8,128)(2,1)} %param.27), kind=kOutput, calls=%fused_computation.60 | convolution fusion | flops 3221618688 | bytes 11272192 | tf_op jit(solution)/shard_map/dot_general | solution.py:146
  257.7 5.6 %all-to-all-start.1 = ((bf16[8,96,512]{2,1,0:T(8,128)(2,1)}), bf16[8,96,512]{2,1,0:T(8,128)(2,1)S(1)}, u32[]{:S(2)}, u32[]{:S(2)}) async-start(bf16[8,96,512]{2,1,0:T(8,128)(2,1)} %bitcast.65), calls=%async_computation.1 | async-start | bytes 1572864 | tf_op jit(solution)/shard_map/all_to_all | solution.py:152
  263.6 20.4 %all-to-all-done.1 = bf16[8,96,512]{2,1,0:T(8,128)(2,1)S(1)} async-done(((bf16[8,96,512]{2,1,0:T(8,128)(2,1)}), bf16[8,96,512]{2,1,0:T(8,128)(2,1)S(1)}, u32[]{:S(2)}, u32[]{:S(2)}) %all-to-all-start.1) | async-done | bytes 786464 | tf_op jit(solution)/shard_map/all_to_all | solution.py:152
  283.9 2.6 gather_fusion.1
  286.5 1.5 reshape.153
  288.0 1.0 multiply_reduce_fusion
  289.0 0.7 add_convert_fusion
  (74 shorter events, 1.2 us)
Async XLA Ops:
  6.5 115.8 %copy-start = (bf16[2048,512]{1,0:T(8,128)(2,1)S(1)}, bf16[2048,512]{1,0:T(8,128)(2,1)}, u32[]{:S(2)}) copy-start(bf16[2048,512]{1,0:T(8,128)(2,1)} %param.23) | copy-start | bytes 6291460
  6.5 6.4 %copy-start.5 = (s32[192,2]{0,1:T(2,128)S(1)}, s32[192,2]{0,1:T(2,128)}, u32[]{:S(2)}) copy-start(s32[192,2]{0,1:T(2,128)} %param.28) | copy-start | bytes 4612
  6.5 4.7 %copy-start.2 = (bf16[192,4,128]{2,1,0:T(4,128)(2,1)S(1)}, bf16[192,4,128]{2,1,0:T(4,128)(2,1)}, u32[]{:S(2)}) copy-start(bf16[192,4,128]{2,1,0:T(4,128)(2,1)} %param.18) | copy-start | bytes 589828
  6.5 49.9 %all-gather.5.cloned.1.call-start = ((), (), s32[]{:S(2)}) async-start(), calls=%async_computation.2 | async-start | bytes 1769472 | tf_op jit(solution)/shard_map/all_gather | solution.py:64
  8.4 92.9 %all-gather.7.cloned.1.call-start = ((), (), s32[]{:S(2)}) async-start(), calls=%async_computation.3 | async-start | bytes 1769472 | tf_op jit(solution)/shard_map/all_gather | solution.py:65
  10.1 181.2 %all-gather.9.cloned.1.call-start = ((), (), s32[]{:S(2)}) async-start(), calls=%async_computation.4 | async-start | bytes 3932160 | tf_op jit(solution)/shard_map/all_gather | solution.py:131
  104.0 9.0 %copy-start.6 = (f32[4]{0:T(128)S(1)}, f32[4]{0:T(128)}, u32[]{:S(2)}) copy-start(f32[4]{0:T(128)} %param.21) | copy-start | bytes 52
  104.0 9.5 %copy-start.7 = (f32[128]{0:T(128)S(1)}, f32[128]{0:T(128)}, u32[]{:S(2)}) copy-start(f32[128]{0:T(128)} %param.22) | copy-start | bytes 1540
  107.8 1.4 copy-start.1
  113.0 9.3 %copy-start.3 = (bf16[192,512]{1,0:T(8,128)(2,1)S(1)}, bf16[192,512]{1,0:T(8,128)(2,1)}, u32[]{:S(2)}) copy-start(bf16[192,512]{1,0:T(8,128)(2,1)} %param.17) | copy-start | bytes 589828
  164.5 84.9 %all-gather.11.cloned.1.call-start = ((), (), s32[]{:S(2)}) async-start(), calls=%async_computation.5 | async-start | bytes 7864320 | tf_op jit(solution)/shard_map/all_gather | solution.py:147
  191.2 6.3 %copy-start.8 = (bf16[1,2048,1024]{2,1,0:T(8,128)(2,1)S(1)}, bf16[1,2048,1024]{2,1,0:T(8,128)(2,1)}, u32[]{:S(2)}) copy-start(bf16[1,2048,1024]{2,1,0:T(8,128)(2,1)} %param.25) | copy-start | bytes 12582916
  191.3 6.3 %copy-start.9 = (bf16[8,96,2048]{2,1,0:T(8,128)(2,1)S(1)}, bf16[8,96,2048]{2,1,0:T(8,128)(2,1)}, u32[]{:S(2)}) copy-start(bf16[8,96,2048]{2,1,0:T(8,128)(2,1)} %all-gather.9.cloned.1.call-done) | copy-start | bytes 9437188
  257.7 5.7 %copy-start.4 = (f32[192,2]{0,1:T(2,128)S(1)}, f32[192,2]{0,1:T(2,128)}, u32[]{:S(2)}) copy-start(f32[192,2]{0,1:T(2,128)} %param.29) | copy-start | bytes 4612
  257.7 26.2 %all-to-all-start.1 = ((bf16[8,96,512]{2,1,0:T(8,128)(2,1)}), bf16[8,96,512]{2,1,0:T(8,128)(2,1)S(1)}, u32[]{:S(2)}, u32[]{:S(2)}) async-start(bf16[8,96,512]{2,1,0:T(8,128)(2,1)} %bitcast.65), calls=%async_computation.1 | async-start | bytes 1572864 | tf_op jit(solution)/shard_map/all_to_all | solution.py:152
Sparse Core Ops, SparseCore 0:
  9.5 46.9 all-gather.4
  58.7 42.5 all-gather.6
  164.6 26.5 all-gather.8
  203.0 46.3 all-gather.10
where the time goes:
time: 297 us; the launch traced here: 296 us
  waiting for transfers between devices  175 us (59%)
  blocking collectives  47.2 us (16%)
  local copies, waits for them, and re-layouts  24.5 us (8%)
  matrix products  22.8 us (8%)
  between operations  13.4 us (5%)
  starting transfers between devices  5.96 us (2%)
  other arithmetic  5.09 us (2%)
    all_gather x1, waiting for transfers between devices, local(): lax.all_gather(hidden, 'tp', axis=1, tiled=True)  46.5 us
    all_gather x1, waiting for transfers between devices, local(): value_piece = lax.all_gather(value_rows, 'sp', axis=0, tiled=True)  42.2 us
    all_gather x1, waiting for transfers between devices, local(): key_piece = lax.all_gather(key_rows, 'sp', axis=0, tiled=True)  39.5 us
    all_to_all x1, blocking collectives, local(): lax.all_to_all(outgoing, 'sp', split_axis=0, concat_axis=0, tiled=True)  32.5 us
    all_gather x1, waiting for transfers between devices, local(): lax.all_gather(lax.all_to_all(outgoing, 'sp', split_axis=0, concat_axis=0...  26.5 us
    all_to_all x1, waiting for transfers between devices, local(): lax.all_to_all(expert_out, 'sp', split_axis=0, concat_axis=0, tiled=True)  20.4 us
    unnamed x25, local copies, waits for them, and re-layouts  9.82 us
    all_gather x1, blocking collectives, local(): lax.all_gather(attended, 'tp', axis=0, tiled=True)  8.58 us
  transfers between devices with their start and end apart: 5, of which 5 were waited for; matrix products, arithmetic and copies ran while one was open for 4% of the time, Pallas kernels for 0%

commit v1 on v0

--- a/solution.py
+++ b/solution.py
@@ -61,7 +61,12 @@
         jnp.zeros((heads_here, tokens_here, value_width), jnp.float32),
     )
     folded = (empty_map, empty_map)
-    key_piece = lax.all_gather(key_rows, "sp", axis=0, tiled=True)
+    ring = [key_rows]
+    for hop in range(7):
+        ring.append(lax.ppermute(ring[-1], "sp", [(dev, (dev + 1) % 8) for dev in range(8)]))
+    key_piece = jnp.roll(
+        jnp.concatenate(ring[::-1], axis=0), (lax.axis_index("sp") + 1) * ring[0].shape[0], axis=0
+    )
     value_piece = lax.all_gather(value_rows, "sp", axis=0, tiled=True)
     key_count = key_piece.shape[0]
     key_width = math.gcd(key_count, 1024)

time: 297 us -> 278 us (0.936)
  waiting for transfers between devices: 175 us -> 146 us
  local copies, waits for them, and re-layouts: 24.5 us -> 33.6 us
    ppermute x0 -> x7, waiting for transfers between devices: none -> 52 us  [local(): lax.ppermute(ring[-1], 'sp', [(dev, (dev + 1) % 8) for dev in range(8)])]
    all_gather x1, waiting for transfers between devices: 42.2 us -> 0.01 us  [local(): value_piece = lax.all_gather(value_rows, 'sp', axis=0, tiled=True)]
    all_gather x1 -> x0, waiting for transfers between devices: 39.5 us -> none  [local(): key_piece = lax.all_gather(key_rows, 'sp', axis=0, tiled=True)]
    unnamed x25 -> x40, local copies, waits for them, and re-layouts: 9.82 us -> 15.8 us
    ppermute x0 -> x7, starting transfers between devices: none -> 3.04 us  [local(): lax.ppermute(ring[-1], 'sp', [(dev, (dev + 1) % 8) for dev in range(8)])]
  transfers between devices with their start and end apart: 5 -> 11, of which waited for: 5 -> 10; matrix products, arithmetic and copies ran while one was open for 4% -> 8% of each run, Pallas kernels for 0% -> 0%
where the time goes in v1:
time: 278 us
  waiting for transfers between devices  146 us (53%)
  blocking collectives  44.9 us (16%)
  local copies, waits for them, and re-layouts  33.6 us (12%)
  matrix products  22.8 us (8%)
  between operations  13.5 us (5%)
  starting transfers between devices  8.82 us (3%)
  other arithmetic  5.77 us (2%)
    ppermute x7, waiting for transfers between devices, local(): lax.ppermute(ring[-1], 'sp', [(dev, (dev + 1) % 8) for dev in range(8)])  52 us
    all_gather x1, waiting for transfers between devices, local(): lax.all_gather(hidden, 'tp', axis=1, tiled=True)  46.5 us
    all_to_all x1, blocking collectives, local(): lax.all_to_all(outgoing, 'sp', split_axis=0, concat_axis=0, tiled=True)  30.2 us
    all_gather x1, waiting for transfers between devices, local(): lax.all_gather(lax.all_to_all(outgoing, 'sp', split_axis=0, concat_axis=0...  27 us
    all_to_all x1, waiting for transfers between devices, local(): lax.all_to_all(expert_out, 'sp', split_axis=0, concat_axis=0, tiled=True)  20.4 us
    unnamed x40, local copies, waits for them, and re-layouts  15.8 us
    all_gather x1, blocking collectives, local(): lax.all_gather(attended, 'tp', axis=0, tiled=True)  8.61 us
    dot_general x1, matrix products, local(): jnp.dot(lax.all_gather(hidden, 'tp', axis=1, tiled=True), weight_slice, p...  8.3 us
  transfers between devices with their start and end apart: 11, of which 10 were waited for; matrix products, arithmetic and copies ran while one was open for 8% of the time, Pallas kernels for 0%

profile of v1, /device:TPU:0, one launch (start us, length us, event | category | flops | bytes accessed | tf_op | source)
XLA Modules:
  0.0 277.5 jit_solution(3017264992284718783)
XLA Ops:
  6.5 1.1 copy.29
  7.7 3.0 %collective-permute-start = (bf16[192,4,128]{2,0,1:T(8,128)(2,1)S(1)}, bf16[192,4,128]{2,0,1:T(8,128)(2,1)S(1)}, u32[]{:S(2)}, u32[]{:S(2)}) collective-permute-start(bf16[192,4,128]{2,0,1:T(8,128)(2,1)S(1)} %copy.29), channel_id=1, source_target_pairs={{0,4},{4,8},{8,12},{12,16},{16,20},{20,24},{24,28},{28,0},{1,5},{5... | collective-permute-start | bytes 589832 | tf_op jit(solution)/shard_map/ppermute | solution.py:66
  10.7 1.6 copy.33
  12.4 0.8 copy.38
  13.5 0.9 reduce-window.6
  14.4 4.3 %collective-permute-done = bf16[192,4,128]{2,0,1:T(8,128)(2,1)S(1)} collective-permute-done((bf16[192,4,128]{2,0,1:T(8,128)(2,1)S(1)}, bf16[192,4,128]{2,0,1:T(8,128)(2,1)S(1)}, u32[]{:S(2)}, u32[]{:S(2)}) %collective-permute-start) | collective-permute-done | bytes 196640 | tf_op jit(solution)/shard_map/ppermute | solution.py:66
  18.6 0.7 broadcast_multiply_fusion
  19.3 10.1 %collective-permute-done.1 = bf16[192,4,128]{2,0,1:T(8,128)(2,1)S(1)} collective-permute-done((bf16[192,4,128]{2,0,1:T(8,128)(2,1)S(1)}, bf16[192,4,128]{2,0,1:T(8,128)(2,1)S(1)}, u32[]{:S(2)}, u32[]{:S(2)}) %collective-permute-start.1) | collective-permute-done | bytes 196640 | tf_op jit(solution)/shard_map/ppermute | solution.py:66
  30.0 7.9 %collective-permute-done.2 = bf16[192,4,128]{2,0,1:T(8,128)(2,1)S(1)} collective-permute-done((bf16[192,4,128]{2,0,1:T(8,128)(2,1)S(1)}, bf16[192,4,128]{2,0,1:T(8,128)(2,1)S(1)}, u32[]{:S(2)}, u32[]{:S(2)}) %collective-permute-start.2) | collective-permute-done | bytes 196640 | tf_op jit(solution)/shard_map/ppermute | solution.py:66
  37.9 1.9 fusion.56
  39.9 6.7 %collective-permute-done.3 = bf16[192,4,128]{2,0,1:T(8,128)(2,1)S(1)} collective-permute-done((bf16[192,4,128]{2,0,1:T(8,128)(2,1)S(1)}, bf16[192,4,128]{2,0,1:T(8,128)(2,1)S(1)}, u32[]{:S(2)}, u32[]{:S(2)}) %collective-permute-start.3) | collective-permute-done | bytes 196640 | tf_op jit(solution)/shard_map/ppermute | solution.py:66
  46.5 12.4 %collective-permute-done.4 = bf16[192,4,128]{2,0,1:T(8,128)(2,1)S(1)} collective-permute-done((bf16[192,4,128]{2,0,1:T(8,128)(2,1)S(1)}, bf16[192,4,128]{2,0,1:T(8,128)(2,1)S(1)}, u32[]{:S(2)}, u32[]{:S(2)}) %collective-permute-start.4) | collective-permute-done | bytes 196640 | tf_op jit(solution)/shard_map/ppermute | solution.py:66
  59.0 2.9 %scatter_custom_fusion = s32[768]{0:T(1024)S(1)} fusion(s32[384]{0:T(512)S(1)} %fusion.51, s32[384]{0:T(512)S(1)} %add_select_fusion.1, s32[]{:T(128)} %constant.159.clone.1), kind=kCustom, calls=%fused_computation.106 | custom fusion | bytes 3076 | tf_op jit(solution)/shard_map/scatter | solution.py:132
  61.9 5.5 %collective-permute-done.5 = bf16[192,4,128]{2,0,1:T(8,128)(2,1)} collective-permute-done((bf16[192,4,128]{2,0,1:T(8,128)(2,1)S(1)}, bf16[192,4,128]{2,0,1:T(8,128)(2,1)}, u32[]{:S(2)}, u32[]{:S(2)}) %collective-permute-start.5) | collective-permute-done | bytes 196640 | tf_op jit(solution)/shard_map/ppermute | solution.py:66
  67.5 1.1 copy.41
  68.5 1.7 copy.42
  70.3 0.8 dynamic_slice.33
  71.0 5.1 %collective-permute-done.6 = bf16[192,4,128]{2,0,1:T(8,128)(2,1)} collective-permute-done((bf16[192,4,128]{2,0,1:T(8,128)(2,1)}, bf16[192,4,128]{2,0,1:T(8,128)(2,1)}, u32[]{:S(2)}, u32[]{:S(2)}) %collective-permute-start.6) | collective-permute-done | bytes 196640 | tf_op jit(solution)/shard_map/ppermute | solution.py:66
  76.1 0.9 constant_dynamic-update-slice_fusion.15
  77.1 1.0 constant_dynamic-update-slice_fusion.14
  78.3 1.0 constant_dynamic-update-slice_fusion.7
  79.3 1.0 constant_dynamic-update-slice_fusion.6
  80.4 1.6 constant_dynamic-slice_fusion
  82.0 2.6 copy.35
  84.6 2.6 copy.36
  87.4 8.8 %while.23 = (s32[]{:T(128)}, f32[4,192]{1,0:T(4,128)S(1)}, f32[4,192]{1,0:T(4,128)S(1)}, f32[4,192,128]{2,1,0:T(8,128)S(1)}, f32[4,192]{1,0:T(4,128)S(1)}, /*ind...) while((s32[]{:T(128)}, f32[4,192]{1,0:T(4,128)S(1)}, ...), condition=%wide.region_7.8_spmd.clone, body=%wide.region_0.7_spmd.clone.sunk | while | flops 309574784 | bytes 20891532 | solution.py:93
  87.5 0.6 dynamic_slice.48
  88.7 4.8 %conditional.3 = ((f32[4,192]{1,0:T(4,128)S(1)}, f32[4,192]{1,0:T(4,128)S(1)}, f32[4,192,128]{2,1,0:T(8,128)S(1)}, f32[4,192]{1,0:T(4,128)S(1)}, f32[4,192]{1,0:T(4,128)S(1)}, /*index=5*/f32[4,192,128]{2,1,0:T(8,128)S(1)})) conditional(s32[]{:T(128)} %convert_element_type.82, (f32[4,192]{1,0:T(4,128)S(1)}, f32[4,192]{1,0:T(4,128)S(1)}, ...), branch_computations={%region_1.1_spmd, %region_2.6_spmd.clone} | conditional | flops 309572096 | bytes 20887848 | solution.py:88
  88.9 1.1 dynamic-slice_bitcast_fusion
  91.2 1.2 fusion.5
  93.6 0.6 dynamic_slice.48
  95.0 0.6 dynamic_slice.48
  97.0 8.6 %all_gather.13 = bf16[16,192,128]{2,1,0:T(8,128)(2,1)S(1)} all-gather(bf16[4,192,128]{2,1,0:T(8,128)(2,1)S(1)} %multiply_convert_fusion.2), channel_id=1, replica_groups=mesh['sp'=8,'tp'=4] {'tp'}, dimensions={0}, use_global_device_ids=true | all-gather | bytes 983040 | tf_op jit(solution)/shard_map/all_gather | solution.py:108
  105.6 0.7 multiply_reduce_fusion.1
  106.3 6.1 %psum.7 = f32[192]{0:T(256)S(1)} all-reduce(f32[192]{0:T(256)S(1)} %get-tuple-element.467), channel_id=1, replica_groups=mesh['sp'=8,'tp'=4] {'tp'}, use_global_device_ids=true, to_apply=%region_10.11 | all-reduce | flops 192 | bytes 1536 | tf_op jit(solution)/shard_map/psum | solution.py:115
  112.5 2.7 gather_fusion
  115.2 30.2 %all_to_all.10 = bf16[8,96,512]{2,1,0:T(8,128)(2,1)} all-to-all(bf16[8,96,512]{2,1,0:T(8,128)(2,1)S(1)} %bitcast.63), channel_id=1, replica_groups=mesh['sp'=8,'tp'=4] {'sp'}, dimensions={0} | all-to-all | bytes 1572864 | tf_op jit(solution)/shard_map/all_to_all | solution.py:137
  145.6 27.0 %all-gather.6.cloned.1.call-done = bf16[8,96,2048]{2,1,0:T(8,128)(2,1)} async-done(((bf16[8,96,512]{2,1,0:T(8,128)(2,1)}), bf16[8,96,2048]{2,1,0:T(8,128)(2,1)}) %all-gather.6.cloned.1.call-update) | async-done | bytes 3145744 | tf_op jit(solution)/shard_map/all_gather | solution.py:136
  172.6 6.3 %fusion.32 = f32[768,1024]{1,0:T(8,128)S(1)} fusion(bf16[768,2048]{1,0:T(8,128)(2,1)} %bitcast.67, bf16[1,2048,1024]{2,1,0:T(8,128)(2,1)} %param.26), kind=kOutput, calls=%fused_computation.55 | convolution fusion | flops 3221225472 | bytes 10485760 | tf_op jit(solution)/shard_map/dot_general | solution.py:146
  179.0 5.3 %multiply_convert_fusion = bf16[768,1024]{1,0:T(8,128)(2,1)} fusion(f32[768,1024]{1,0:T(8,128)S(1)} %fusion.32, bf16[768,2048]{1,0:T(8,128)(2,1)S(1)} %bitcast.68, bf16[1,2048,1024]{2,1,0:T(8,128)(2,1)S(1)} %copy-done.8), kind=kOutput, calls=%fused_computation.59 | convolution fusion | flops 3229089792 | bytes 12058624 | tf_op jit(solution)/shard_map/dot_general | solution.py:145
  184.3 46.5 %all-gather.8.cloned.1.call-done = bf16[768,4096]{1,0:T(8,128)(2,1)} async-done(((bf16[768,1024]{1,0:T(8,128)(2,1)}), bf16[768,4096]{1,0:T(8,128)(2,1)}) %all-gather.8.cloned.1.call-update) | async-done | bytes 6291472 | tf_op jit(solution)/shard_map/all_gather | solution.py:152
  230.8 8.3 %fusion.38 = bf16[768,512]{1,0:T(8,128)(2,1)} fusion(bf16[768,4096]{1,0:T(8,128)(2,1)} %all-gather.8.cloned.1.call-done, bf16[1,4096,512]{2,1,0:T(8,128)(2,1)} %param.27), kind=kOutput, calls=%fused_computation.60 | convolution fusion | flops 3221618688 | bytes 11272192 | tf_op jit(solution)/shard_map/dot_general | solution.py:151
  239.1 5.5 %all-to-all-start.1 = ((bf16[8,96,512]{2,1,0:T(8,128)(2,1)}), bf16[8,96,512]{2,1,0:T(8,128)(2,1)S(1)}, u32[]{:S(2)}, u32[]{:S(2)}) async-start(bf16[8,96,512]{2,1,0:T(8,128)(2,1)} %bitcast.65), calls=%async_computation.1 | async-start | bytes 1572864 | tf_op jit(solution)/shard_map/all_to_all | solution.py:157
  244.8 20.4 %all-to-all-done.1 = bf16[8,96,512]{2,1,0:T(8,128)(2,1)S(1)} async-done(((bf16[8,96,512]{2,1,0:T(8,128)(2,1)}), bf16[8,96,512]{2,1,0:T(8,128)(2,1)S(1)}, u32[]{:S(2)}, u32[]{:S(2)}) %all-to-all-start.1) | async-done | bytes 786464 | tf_op jit(solution)/shard_map/all_to_all | solution.py:157
  265.2 2.6 gather_fusion.1
  267.8 1.5 reshape.153
  269.3 1.0 multiply_reduce_fusion
  270.3 0.7 add_convert_fusion
  (102 shorter events, 5.3 us)
Async XLA Ops:
  6.5 99.0 %copy-start = (bf16[2048,512]{1,0:T(8,128)(2,1)S(1)}, bf16[2048,512]{1,0:T(8,128)(2,1)}, u32[]{:S(2)}) copy-start(bf16[2048,512]{1,0:T(8,128)(2,1)} %param.23) | copy-start | bytes 6291460
  6.5 71.7 %copy-start.2 = (bf16[192,4,128]{2,1,0:T(4,128)(2,1)S(1)}, bf16[192,4,128]{2,1,0:T(4,128)(2,1)}, u32[]{:S(2)}) copy-start(bf16[192,4,128]{2,1,0:T(4,128)(2,1)} %param.19) | copy-start | bytes 589828
  6.5 78.1 %all-gather.4.cloned.1.call-start = ((), (), s32[]{:S(2)}) async-start(), calls=%async_computation.2 | async-start | bytes 1769472 | tf_op jit(solution)/shard_map/all_gather | solution.py:70
  7.7 11.0 %collective-permute-start = (bf16[192,4,128]{2,0,1:T(8,128)(2,1)S(1)}, bf16[192,4,128]{2,0,1:T(8,128)(2,1)S(1)}, u32[]{:S(2)}, u32[]{:S(2)}) collective-permute-start(bf16[192,4,128]{2,0,1:T(8,128)(2,1)S(1)} %copy.29), channel_id=1, source_target_pairs={{0,4},{4,8},{8,12},{12,16},{16,20},{20,24},{24,28},{28,0},{1,5},{5... | collective-permute-start | bytes 589832 | tf_op jit(solution)/shard_map/ppermute | solution.py:66
  12.3 160.3 %all-gather.6.cloned.1.call-start = ((), (), s32[]{:S(2)}) async-start(), calls=%async_computation.3 | async-start | bytes 3932160 | tf_op jit(solution)/shard_map/all_gather | solution.py:136
  18.6 10.8 %collective-permute-start.1 = (bf16[192,4,128]{2,0,1:T(8,128)(2,1)S(1)}, bf16[192,4,128]{2,0,1:T(8,128)(2,1)S(1)}, u32[]{:S(2)}, u32[]{:S(2)}) collective-permute-start(bf16[192,4,128]{2,0,1:T(8,128)(2,1)S(1)} %collective-permute-done), channel_id=1, source_target_pairs={{0,4},{4,8},{8,12},{12,16},{16,20},{20,24},{24,28},{28,0},{1,5},{5... | collective-permute-start | bytes 589832 | tf_op jit(solution)/shard_map/ppermute | solution.py:66
  29.4 8.5 %collective-permute-start.2 = (bf16[192,4,128]{2,0,1:T(8,128)(2,1)S(1)}, bf16[192,4,128]{2,0,1:T(8,128)(2,1)S(1)}, u32[]{:S(2)}, u32[]{:S(2)}) collective-permute-start(bf16[192,4,128]{2,0,1:T(8,128)(2,1)S(1)} %collective-permute-done.1), channel_id=1, source_target_pairs={{0,4},{4,8},{8,12},{12,16},{16,20},{20,24},{24,28},{28,0},{1,5},{5... | collective-permute-start | bytes 589832 | tf_op jit(solution)/shard_map/ppermute | solution.py:66
  37.9 8.6 %collective-permute-start.3 = (bf16[192,4,128]{2,0,1:T(8,128)(2,1)S(1)}, bf16[192,4,128]{2,0,1:T(8,128)(2,1)S(1)}, u32[]{:S(2)}, u32[]{:S(2)}) collective-permute-start(bf16[192,4,128]{2,0,1:T(8,128)(2,1)S(1)} %collective-permute-done.2), channel_id=1, source_target_pairs={{0,4},{4,8},{8,12},{12,16},{16,20},{20,24},{24,28},{28,0},{1,5},{5... | collective-permute-start | bytes 589832 | tf_op jit(solution)/shard_map/ppermute | solution.py:66
  46.5 12.4 %collective-permute-start.4 = (bf16[192,4,128]{2,0,1:T(8,128)(2,1)S(1)}, bf16[192,4,128]{2,0,1:T(8,128)(2,1)S(1)}, u32[]{:S(2)}, u32[]{:S(2)}) collective-permute-start(bf16[192,4,128]{2,0,1:T(8,128)(2,1)S(1)} %collective-permute-done.3), channel_id=1, source_target_pairs={{0,4},{4,8},{8,12},{12,16},{16,20},{20,24},{24,28},{28,0},{1,5},{5... | collective-permute-start | bytes 589832 | tf_op jit(solution)/shard_map/ppermute | solution.py:66
  59.0 8.5 %collective-permute-start.5 = (bf16[192,4,128]{2,0,1:T(8,128)(2,1)S(1)}, bf16[192,4,128]{2,0,1:T(8,128)(2,1)}, u32[]{:S(2)}, u32[]{:S(2)}) collective-permute-start(bf16[192,4,128]{2,0,1:T(8,128)(2,1)S(1)} %collective-permute-done.4), channel_id=1, source_target_pairs={{0,4},{4,8},{8,12},{12,16},{16,20},{20,24},{24,28},{28,0},{1,5},{5... | collective-permute-start | bytes 589832 | tf_op jit(solution)/shard_map/ppermute | solution.py:66
  67.5 8.7 %collective-permute-start.6 = (bf16[192,4,128]{2,0,1:T(8,128)(2,1)}, bf16[192,4,128]{2,0,1:T(8,128)(2,1)}, u32[]{:S(2)}, u32[]{:S(2)}) collective-permute-start(bf16[192,4,128]{2,0,1:T(8,128)(2,1)} %collective-permute-done.5), channel_id=1, source_target_pairs={{0,4},{4,8},{8,12},{12,16},{16,20},{20,24},{24,28},{28,0},{1,5},{5... | collective-permute-start | bytes 589832 | tf_op jit(solution)/shard_map/ppermute | solution.py:66
  82.0 5.4 %copy-start.4 = (bf16[192,4,64]{0,2,1:T(8,128)(2,1)S(1)}, bf16[192,4,64]{0,2,1:T(8,128)(2,1)}, u32[]{:S(2)}) copy-start(bf16[192,4,64]{0,2,1:T(8,128)(2,1)} %copy.42) | copy-start | bytes 294916
  87.4 8.9 %copy-start.6 = (f32[4]{0:T(128)S(1)}, f32[4]{0:T(128)}, u32[]{:S(2)}) copy-start(f32[4]{0:T(128)} %param.21) | copy-start | bytes 52
  87.4 9.4 %copy-start.7 = (f32[128]{0:T(128)S(1)}, f32[128]{0:T(128)}, u32[]{:S(2)}) copy-start(f32[128]{0:T(128)} %param.22) | copy-start | bytes 1540
  87.4 18.2 %copy-start.3 = (bf16[192,512]{1,0:T(8,128)(2,1)S(1)}, bf16[192,512]{1,0:T(8,128)(2,1)}, u32[]{:S(2)}) copy-start(bf16[192,512]{1,0:T(8,128)(2,1)} %param.17) | copy-start | bytes 589828
  90.6 1.8 copy-start.1
  145.4 85.4 %all-gather.8.cloned.1.call-start = ((), (), s32[]{:S(2)}) async-start(), calls=%async_computation.4 | async-start | bytes 7864320 | tf_op jit(solution)/shard_map/all_gather | solution.py:152
  172.6 6.3 %copy-start.8 = (bf16[1,2048,1024]{2,1,0:T(8,128)(2,1)S(1)}, bf16[1,2048,1024]{2,1,0:T(8,128)(2,1)}, u32[]{:S(2)}) copy-start(bf16[1,2048,1024]{2,1,0:T(8,128)(2,1)} %param.25) | copy-start | bytes 12582916
  172.6 6.3 %copy-start.9 = (bf16[8,96,2048]{2,1,0:T(8,128)(2,1)S(1)}, bf16[8,96,2048]{2,1,0:T(8,128)(2,1)}, u32[]{:S(2)}) copy-start(bf16[8,96,2048]{2,1,0:T(8,128)(2,1)} %all-gather.6.cloned.1.call-done) | copy-start | bytes 9437188
  184.3 60.3 %copy-start.5 = (f32[192,2]{0,1:T(2,128)S(1)}, f32[192,2]{0,1:T(2,128)}, u32[]{:S(2)}) copy-start(f32[192,2]{0,1:T(2,128)} %param.29) | copy-start | bytes 4612
  239.1 26.1 %all-to-all-start.1 = ((bf16[8,96,512]{2,1,0:T(8,128)(2,1)}), bf16[8,96,512]{2,1,0:T(8,128)(2,1)S(1)}, u32[]{:S(2)}, u32[]{:S(2)}) async-start(bf16[8,96,512]{2,1,0:T(8,128)(2,1)} %bitcast.65), calls=%async_computation.1 | async-start | bytes 1572864 | tf_op jit(solution)/shard_map/all_to_all | solution.py:157
Sparse Core Ops, SparseCore 0:
  12.5 51.0 all-gather.3
  145.5 27.0 all-gather.5
  184.4 46.3 all-gather.7
